TPU v7x, 32 devices: a whole 2x2x4 slice. The times are simulated.
32 devices in a mesh: grp: 2 (over y), fs: 4 (over z), tp: 4 (over x, core).
Axes of the slice: x: 2, y: 2, z: 4, core: 2. Of those that a mesh axis runs over, the one named last changes fastest.
Arguments:
- layer_input_tokens: bfloat16 [4096, 2048], P(('grp', 'fs')), parts along dimension 0, may hold values from -6 to 6
- attention_norm_gain: float32 [2048], replicated, may hold values from 0.1 to 1.9
- query_projection: bfloat16 [2048, 1024], P('fs', 'tp'), may hold values from -0.125 to 0.125
- key_projection: bfloat16 [2048, 1024], P('fs', 'tp'), may hold values from -0.125 to 0.125
- value_projection: bfloat16 [2048, 2048], P('fs', 'tp'), may hold values from -0.125 to 0.125
- decay_first_factor: bfloat16 [2048, 16], replicated, may hold values from -0.125 to 0.125
- decay_second_factor: bfloat16 [16, 1024], P(None, 'tp'), may hold values from -1.5 to 1.5
- decay_logit_bias: float32 [1024], P('tp'), may hold values from -0.5 to 6
- extra_log_decay: float32 [4096, 8], P(('grp', 'fs'), 'tp'), parts along dimension 0, may hold values from -0.7 to 0
- head_output_gain: float32 [256], replicated, may hold values from 0.1 to 1.9
- attention_output_projection: bfloat16 [2048, 2048], P(('tp', 'fs')), may hold values from -0.125 to 0.125
- feedforward_norm_gain: float32 [2048], replicated, may hold values from 0.1 to 1.9
- gate_projection: bfloat16 [2048, 5632], P('fs', 'tp'), may hold values from -0.125 to 0.125
- up_projection: bfloat16 [2048, 5632], P('fs', 'tp'), may hold values from -0.125 to 0.125
- down_projection: bfloat16 [5632, 2048], P(('tp', 'fs')), may hold values from -0.078125 to 0.078125
Outputs:
- result: bfloat16 [4096, 2048], P(('grp', 'fs')), parts along dimension 0
There are 2 independent parts, one for each index of `grp`. A program takes and returns all parts, laid end to end along the dimension named above; an argument that names none is the same for every part. Nothing has to cross between parts.
All inputs are finite; a program needn't handle non-finite values.
Results may differ from a plain program's by a relative error of at most 0.02.
Values may be sent and summed in bfloat16 or wider, within the bound.
A program may use at most 64 MiB of HBM per device.

v0:
```python
import jax
import jax.numpy as jnp
from jax import lax
from jax.sharding import PartitionSpec as P

BLOCK = 64
normed_gate = 16.0


def norm_rows(values, gain):
    wide = values.astype(jnp.float32)
    scale = lax.rsqrt(jnp.mean(wide * wide, axis=-1, keepdims=True) + 1e-06)
    return wide * scale * gain


def block_scan(queries, keys, values, decays):
    length, key_channel_width = queries.shape
    value_width = values.shape[1]
    count = length // BLOCK
    lower_mask = jnp.arange(BLOCK)[:, None] >= jnp.arange(BLOCK)[None, :]

    def advance(carry, items):
        query_block, key_block, value_block, decay_block = items
        running = jnp.cumsum(decay_block, axis=0)
        middle = running[BLOCK // 2 - 1]
        closing = running[BLOCK - 1]
        carried = jnp.dot(query_block * jnp.exp(running), carry, precision=lax.Precision.HIGHEST)
        scores = jnp.dot(
            query_block * jnp.exp(running - middle),
            (key_block * jnp.exp(middle - running)).T,
            precision=lax.Precision.HIGHEST,
        )
        scores = jnp.where(lower_mask, scores, 0.0)
        inside = jnp.dot(scores, value_block, precision=lax.Precision.HIGHEST)
        fresh = carry * jnp.exp(closing)[:, None] + jnp.dot(
            (key_block * jnp.exp(closing - running)).T, value_block, precision=lax.Precision.HIGHEST
        )
        return (fresh, carried + inside)

    items = (
        queries.reshape(count, BLOCK, key_channel_width),
        keys.reshape(count, BLOCK, key_channel_width),
        values.reshape(count, BLOCK, value_width),
        decays.reshape(count, BLOCK, key_channel_width),
    )
    _, outputs = lax.scan(advance, jnp.zeros((key_channel_width, value_width), jnp.float32), items)
    return outputs.reshape(length, value_width)


def both_ways(queries, keys, values, decays):
    ahead = block_scan(queries, keys, values, decays)
    behind = block_scan(
        jnp.flip(queries, 0), jnp.flip(keys, 0), jnp.flip(values, 0), jnp.flip(decays, 0)
    )
    return ahead + jnp.flip(behind, 0)


def head_norm(mixed, gain):
    scale = lax.rsqrt(jnp.mean(mixed * mixed, axis=-1, keepdims=True) + 1e-06)
    return mixed * scale * gain


def shards(
    layer_input_tokens,
    attention_norm_gain,
    query_projection,
    key_projection,
    value_projection,
    decay_first_factor,
    decay_second_factor,
    decay_logit_bias,
    extra_log_decay,
    head_output_gain,
    attention_output_projection,
    feedforward_norm_gain,
    gate_projection,
    up_projection,
    down_projection,
):
    rows = layer_input_tokens.shape[0]
    normed = norm_rows(layer_input_tokens, attention_norm_gain).astype(jnp.bfloat16)
    pieces = (
        lax.all_gather(query_projection, "fs", axis=0, tiled=True),
        lax.all_gather(key_projection, "fs", axis=0, tiled=True),
        lax.all_gather(value_projection, "fs", axis=0, tiled=True),
    )
    query, key, value = tuple(
        (jnp.dot(normed, piece, preferred_element_type=jnp.float32) for piece in pieces)
    )
    query = query.astype(jnp.bfloat16)
    key = key.astype(jnp.bfloat16)
    value = value.astype(jnp.bfloat16)
    lowrank = jnp.dot(normed, decay_first_factor, preferred_element_type=jnp.float32).astype(
        jnp.bfloat16
    )
    decay_logit_values = (
        jnp.dot(lowrank, decay_second_factor, preferred_element_type=jnp.float32) + decay_logit_bias
    )
    local_heads = extra_log_decay.shape[1]
    key_channel_width = query.shape[1] // local_heads
    value_width = value.shape[1] // local_heads
    decay_logarithm = jax.nn.log_sigmoid(decay_logit_values) / normed_gate + jnp.repeat(
        extra_log_decay, key_channel_width, axis=1
    )
    mixed = jax.vmap(both_ways, in_axes=1, out_axes=1)(
        query.astype(jnp.float32).reshape(rows, local_heads, key_channel_width),
        key.astype(jnp.float32).reshape(rows, local_heads, key_channel_width),
        value.astype(jnp.float32).reshape(rows, local_heads, value_width),
        decay_logarithm.reshape(rows, local_heads, key_channel_width),
    )
    headed = (
        head_norm(mixed, head_output_gain)
        .reshape(rows, local_heads * value_width)
        .astype(jnp.bfloat16)
    )
    share = rows // lax.axis_size("tp")
    out_full = lax.all_gather(attention_output_projection, "fs", axis=0, tiled=True)
    mixer = lax.psum_scatter(
        jnp.dot(headed, out_full, preferred_element_type=jnp.float32).astype(jnp.bfloat16),
        "tp",
        scatter_dimension=0,
        tiled=True,
    ).astype(jnp.float32)
    own = lax.dynamic_slice_in_dim(layer_input_tokens, lax.axis_index("tp") * share, share, 0)
    residual = (own.astype(jnp.float32) + mixer).astype(jnp.bfloat16)
    second = lax.all_gather(
        norm_rows(residual, feedforward_norm_gain).astype(jnp.bfloat16), "tp", axis=0, tiled=True
    )
    gate_full, up_full = (
        lax.all_gather(gate_projection, "fs", axis=0, tiled=True),
        lax.all_gather(up_projection, "fs", axis=0, tiled=True),
    )
    gate = jnp.dot(second, gate_full, preferred_element_type=jnp.float32)
    up = jnp.dot(second, up_full, preferred_element_type=jnp.float32)
    hidden = (jax.nn.silu(gate) * up).astype(jnp.bfloat16)
    down_full = lax.all_gather(down_projection, "fs", axis=0, tiled=True)
    channel = lax.psum_scatter(
        jnp.dot(hidden, down_full, preferred_element_type=jnp.float32).astype(jnp.bfloat16),
        "tp",
        scatter_dimension=0,
        tiled=True,
    ).astype(jnp.float32)
    finished = (residual.astype(jnp.float32) + channel).astype(jnp.bfloat16)
    return lax.all_gather(finished, "tp", axis=0, tiled=True)


def solution(mesh):
    placed = (
        P(("grp", "fs"), None),
        P(),
        P("fs", "tp"),
        P("fs", "tp"),
        P("fs", "tp"),
        P(),
        P(None, "tp"),
        P("tp"),
        P(("grp", "fs"), "tp"),
        P(),
        P(("tp", "fs"), None),
        P(),
        P("fs", "tp"),
        P("fs", "tp"),
        P(("tp", "fs"), None),
    )
    return jax.shard_map(
        shards, mesh=mesh, in_specs=placed, out_specs=P(("grp", "fs"), None), check_vma=False
    )
```

profile of v0, /device:TPU:0, one launch (start us, length us, event | category | flops | bytes accessed | tf_op | source)
XLA Modules:
  0.0 674.9 jit_solution(432019829572898455)
XLA Ops:
  9.4 2.1 fusion.60
  11.6 2.0 fusion.74
  14.8 2.7 rev.18
  17.5 22.2 %all-gather.10.cloned.1.call-done = bf16[2048,256]{1,0:T(8,128)(2,1)} async-done(((bf16[512,256]{1,0:T(8,128)(2,1)}), bf16[2048,256]{1,0:T(8,128)(2,1)}) %all-gather.10.cloned.1.call-update) | async-done | bytes 1048592 | tf_op jit(solution)/shard_map/all_gather | solution.py:84
  39.7 2.1 convolution_convert_fusion.4
  42.0 2.6 rev.19
  44.6 24.1 %all-gather.14.cloned.1.call-done = bf16[2048,256]{1,0:T(8,128)(2,1)} async-done(((bf16[512,256]{1,0:T(8,128)(2,1)}), bf16[2048,256]{1,0:T(8,128)(2,1)}) %all-gather.14.cloned.1.call-update) | async-done | bytes 1048592 | tf_op jit(solution)/shard_map/all_gather | solution.py:83
  68.6 2.1 convolution_convert_fusion.3
  71.7 4.7 rev.21
  76.4 38.8 %all-gather.12.cloned.1.call-done = bf16[2048,512]{1,0:T(8,128)(2,1)} async-done(((bf16[512,512]{1,0:T(8,128)(2,1)}), bf16[2048,512]{1,0:T(8,128)(2,1)}) %all-gather.12.cloned.1.call-update) | async-done | bytes 2097168 | tf_op jit(solution)/shard_map/all_gather | solution.py:85
  115.3 3.8 convolution_convert_fusion.2
  120.3 5.1 rev.20
  126.5 51.9 %while.27 = (s32[]{:T(128)}, f32[2,128,256]{2,1,0:T(8,128)S(1)}, f32[8,2,64,256]{3,2,0,1:T(8,128)}, f32[8,2,64,128]{3,2,0,1:T(8,128)}, f32[8,2,64,128]{3,2,0,1:T...) while((s32[]{:T(128)}, f32[2,128,256]{2,1,0:T(8,128)S(1)}, ...), condition=%wide.region_6.7_spmd.clone, body=%wide.region_4.6_spmd.clone.sunk | while | flops 139866112 | bytes 2319992 | solution.py:46
  136.3 1.8 fusion.125
  142.8 1.8 fusion.125
  155.7 1.8 fusion.125
  162.2 1.8 fusion.125
  168.7 1.8 fusion.125
  178.6 31.7 %while.26 = (s32[]{:T(128)}, f32[2,128,256]{2,1,0:T(8,128)S(1)}, f32[8,2,64,256]{3,2,0,1:T(8,128)S(1)}, f32[8,2,64,128]{3,2,0,1:T(8,128)}, f32[8,2,64,128]{3,2,0...) while((s32[]{:T(128)}, f32[2,128,256]{2,1,0:T(8,128)S(1)}, ...), condition=%wide.region_3.4_spmd.clone, body=%wide.region_1.3_spmd.clone.sunk | while | flops 139866112 | bytes 2352760 | solution.py:46
  210.2 6.8 %rev.22 = f32[2,512,256]{2,1,0:T(8,128)S(1)} reverse(f32[2,512,256]{2,1,0:T(8,128)} %bitcast.196), dimensions={1} | reverse | bytes 2097152 | tf_op jit(solution)/shard_map/vmap(jit(_flip))/rev | solution.py:55
  217.9 4.2 convolution_convert_fusion
  222.8 29.6 %reduce-scatter.3.cloned.1.call-done = bf16[128,2048]{1,0:T(8,128)(2,1)} async-done(((bf16[512,2048]{1,0:T(8,128)(2,1)}), bf16[128,2048]{1,0:T(8,128)(2,1)}) %reduce-scatter.3.cloned.1.call-update) | async-done | bytes 524304 | tf_op jit(solution)/shard_map/reduce_scatter | solution.py:118
  256.6 103.9 %all-gather.20.cloned.1.call-done = bf16[2048,1408]{1,0:T(8,128)(2,1)} async-done(((bf16[512,1408]{1,0:T(8,128)(2,1)}), bf16[2048,1408]{1,0:T(8,128)(2,1)}) %all-gather.20.cloned.1.call-update) | async-done | bytes 5767184 | tf_op jit(solution)/shard_map/all_gather | solution.py:130
  360.5 22.4 %all-gather.18.cloned.1.call-done = bf16[512,2048]{1,0:T(8,128)(2,1)} async-done(((bf16[128,2048]{1,0:T(8,128)(2,1)}), bf16[512,2048]{1,0:T(8,128)(2,1)}) %all-gather.18.cloned.1.call-update) | async-done | bytes 2097168 | tf_op jit(solution)/shard_map/all_gather | solution.py:126
  382.9 8.4 %fusion.83 = f32[512,1408]{1,0:T(8,128)} fusion(bf16[512,2048]{1,0:T(8,128)(2,1)} %all-gather.18.cloned.1.call-done, bf16[2048,1408]{1,0:T(8,128)(2,1)} %all-gather.20.cloned.1.call-done), kind=kOutput, calls=%fused_computation.115 | convolution fusion | flops 2952790016 | bytes 10747904 | tf_op jit(solution)/shard_map/dot_general | solution.py:133
  391.3 99.9 %all-gather.22.cloned.1.call-done = bf16[2048,1408]{1,0:T(8,128)(2,1)} async-done(((bf16[512,1408]{1,0:T(8,128)(2,1)}), bf16[2048,1408]{1,0:T(8,128)(2,1)}) %all-gather.22.cloned.1.call-update) | async-done | bytes 5767184 | tf_op jit(solution)/shard_map/all_gather | solution.py:131
  491.2 106.6 %all-gather.24.cloned.1.call-done = bf16[1408,2048]{1,0:T(8,128)(2,1)} async-done(((bf16[352,2048]{1,0:T(8,128)(2,1)}), bf16[1408,2048]{1,0:T(8,128)(2,1)}) %all-gather.24.cloned.1.call-update) | async-done | bytes 5767184 | tf_op jit(solution)/shard_map/all_gather | solution.py:136
  597.8 13.2 %convolution_convert_fusion.1 = bf16[512,2048]{1,0:T(8,128)(2,1)} fusion(bf16[1408,2048]{1,0:T(8,128)(2,1)} %all-gather.24.cloned.1.call-done, bf16[512,2048]{1,0:T(8,128)(2,1)S(1)} %copy-done.9, bf16[2048,1408]{1,0:T(8,128)(2,1)} %all-gather.22.cloned.1.call-done, f32[512,1408]{1,0:T(8,128)} %fusion.83), kind=kOutput, calls=%fused_computation.84 | convolution fusion | flops 5910953984 | bytes 18612224 | tf_op jit(solution)/shard_map/dot_general | solution.py:138
  611.0 29.5 %reduce-scatter.5.cloned.1.call-done = bf16[128,2048]{1,0:T(8,128)(2,1)} async-done(((bf16[512,2048]{1,0:T(8,128)(2,1)}), bf16[128,2048]{1,0:T(8,128)(2,1)}) %reduce-scatter.5.cloned.1.call-update) | async-done | bytes 524304 | tf_op jit(solution)/shard_map/reduce_scatter | solution.py:137
  640.6 2.0 fusion.68
  642.6 22.7 %all-gather.26.cloned.1.call-done = bf16[512,2048]{1,0:T(8,128)(2,1)} async-done(((bf16[128,2048]{1,0:T(8,128)(2,1)}), bf16[512,2048]{1,0:T(8,128)(2,1)}) %all-gather.26.cloned.1.call-update) | async-done | bytes 2097168 | tf_op jit(solution)/shard_map/all_gather | solution.py:144
  665.3 3.2 copy.73
  (199 shorter events, 86.7 us)
Async XLA Ops:
  6.5 5.0 copy-start
  6.5 5.0 copy-start.1
  6.5 5.0 copy-start.4
  6.5 5.0 copy-start.3
  6.5 5.0 copy-start.7
  6.5 5.0 copy-start.6
  6.6 33.1 %all-gather.10.cloned.1.call-start = ((), (), s32[]{:S(2)}) async-start(), calls=%async_computation.2 | async-start | bytes 1310720 | tf_op jit(solution)/shard_map/all_gather | solution.py:84
  7.3 61.3 %all-gather.14.cloned.1.call-start = ((), (), s32[]{:S(2)}) async-start(), calls=%async_computation.4 | async-start | bytes 1310720 | tf_op jit(solution)/shard_map/all_gather | solution.py:83
  8.0 107.2 %all-gather.12.cloned.1.call-start = ((), (), s32[]{:S(2)}) async-start(), calls=%async_computation.3 | async-start | bytes 2621440 | tf_op jit(solution)/shard_map/all_gather | solution.py:85
  8.8 209.2 %all-gather.16.cloned.1.call-start = ((), (), s32[]{:S(2)}) async-start(), calls=%async_computation.5 | async-start | bytes 2621440 | tf_op jit(solution)/shard_map/all_gather | solution.py:117
  9.4 243.0 %reduce-scatter.3.cloned.1.call-start = ((), (), s32[]{:S(2)}) async-start(), calls=%async_computation.6 | async-start | bytes 2621440 | tf_op jit(solution)/shard_map/reduce_scatter | solution.py:118
  14.8 27.0 %copy-start.2 = (f32[512,2,128]{2,0,1:T(8,128)}, f32[512,2,128]{2,0,1:T(8,128)S(1)}, u32[]{:S(2)}) copy-start(f32[512,2,128]{2,0,1:T(8,128)S(1)} %copy.16) | copy-start | bytes 1572868
  210.2 7.2 %copy-start.8 = (f32[256]{0:T(256)S(1)}, f32[256]{0:T(256)}, u32[]{:S(2)}) copy-start(f32[256]{0:T(256)} %param.28) | copy-start | bytes 3076
  222.1 31.7 %copy-start.5 = (f32[2048]{0:T(1024)S(1)}, f32[2048]{0:T(1024)}, u32[]{:S(2)}) copy-start(f32[2048]{0:T(1024)} %param.30) | copy-start | bytes 24580
  222.2 138.3 %all-gather.20.cloned.1.call-start = ((), (), s32[]{:S(2)}) async-start(), calls=%async_computation.8 | async-start | bytes 7208960 | tf_op jit(solution)/shard_map/all_gather | solution.py:130
  222.7 160.2 %all-gather.18.cloned.1.call-start = ((), (), s32[]{:S(2)}) async-start(), calls=%async_computation.7 | async-start | bytes 2621440 | tf_op jit(solution)/shard_map/all_gather | solution.py:126
  254.8 236.4 %all-gather.22.cloned.1.call-start = ((), (), s32[]{:S(2)}) async-start(), calls=%async_computation.9 | async-start | bytes 7208960 | tf_op jit(solution)/shard_map/all_gather | solution.py:131
  255.6 342.2 %all-gather.24.cloned.1.call-start = ((), (), s32[]{:S(2)}) async-start(), calls=%async_computation.10 | async-start | bytes 7208960 | tf_op jit(solution)/shard_map/all_gather | solution.py:136
  256.3 384.2 %reduce-scatter.5.cloned.1.call-start = ((), (), s32[]{:S(2)}) async-start(), calls=%async_computation.11 | async-start | bytes 2621440 | tf_op jit(solution)/shard_map/reduce_scatter | solution.py:137
  382.9 214.8 %copy-start.9 = (bf16[512,2048]{1,0:T(8,128)(2,1)S(1)}, bf16[512,2048]{1,0:T(8,128)(2,1)}, u32[]{:S(2)}) copy-start(bf16[512,2048]{1,0:T(8,128)(2,1)} %all-gather.18.cloned.1.call-done) | copy-start | bytes 6291460
  611.0 54.3 %all-gather.26.cloned.1.call-start = ((), (), s32[]{:S(2)}) async-start(), calls=%async_computation.12 | async-start | bytes 2621440 | tf_op jit(solution)/shard_map/all_gather | solution.py:144
Sparse Core Ops, SparseCore 0:
  8.9 30.6 all-gather.9
  41.2 27.3 all-gather.13
  70.2 45.0 all-gather.11
  116.7 44.4 all-gather.15
  222.3 30.0 reduce-scatter.2
  253.8 106.6 all-gather.19
  362.1 20.8 all-gather.17
  384.5 106.6 all-gather.21
  492.8 104.9 all-gather.23
  611.1 29.4 reduce-scatter.4
  642.7 22.5 all-gather.25
where the time goes:
time: 679 us; the launch traced here: 675 us
  waiting for transfers between devices  504 us (74%)
  matrix products  103 us (15%)
  local copies, waits for them, and re-layouts  43.9 us (6%)
  between operations  13.5 us (2%)
  other arithmetic  8.82 us (1%)
    all_gather x1, waiting for transfers between devices, shards(): down_full = lax.all_gather(down_projection, 'fs', axis=0, tiled=True)  107 us
    all_gather x1, waiting for transfers between devices, shards(): lax.all_gather(gate_projection, 'fs', axis=0, tiled=True)  104 us
    all_gather x1, waiting for transfers between devices, shards(): lax.all_gather(up_projection, 'fs', axis=0, tiled=True)  99.9 us
    all_gather x1, waiting for transfers between devices, shards(): lax.all_gather(value_projection, 'fs', axis=0, tiled=True)  38.8 us
    reduce_scatter x1, waiting for transfers between devices, shards(): lax.psum_scatter(jnp.dot(headed, out_full, preferred_element_type=jnp.flo...  29.6 us
    reduce_scatter x1, waiting for transfers between devices, shards(): lax.psum_scatter(jnp.dot(hidden, down_full, preferred_element_type=jnp.fl...  29.5 us
    all_gather x1, waiting for transfers between devices, shards(): lax.all_gather(query_projection, 'fs', axis=0, tiled=True)  24.1 us
    all_gather x1, waiting for transfers between devices, shards(): return lax.all_gather(finished, 'tp', axis=0, tiled=True)  22.7 us
  transfers between devices with their start and end apart: 11, of which 10 were waited for; matrix products, arithmetic and copies ran while one was open for 20% of the time, Pallas kernels for 0%

commit v1 on v0

--- a/solution.py
+++ b/solution.py
@@ -133,7 +133,12 @@
     gate = jnp.dot(second, gate_full, preferred_element_type=jnp.float32)
     up = jnp.dot(second, up_full, preferred_element_type=jnp.float32)
     hidden = (jax.nn.silu(gate) * up).astype(jnp.bfloat16)
-    down_full = lax.all_gather(down_projection, "fs", axis=0, tiled=True)
+    ring = [down_projection]
+    for hop in range(3):
+        ring.append(lax.ppermute(ring[-1], "fs", [(dev, (dev + 1) % 4) for dev in range(4)]))
+    down_full = jnp.roll(
+        jnp.concatenate(ring[::-1], axis=0), (lax.axis_index("fs") + 1) * ring[0].shape[0], axis=0
+    )
     channel = lax.psum_scatter(
         jnp.dot(hidden, down_full, preferred_element_type=jnp.float32).astype(jnp.bfloat16),
         "tp",

time: 679 us -> 626 us (0.922)
  waiting for transfers between devices: 504 us -> 399 us
  starting transfers between devices: 0.61 us -> 37.1 us
  local copies, waits for them, and re-layouts: 43.9 us -> 59.5 us
    ppermute x0 -> x3, waiting for transfers between devices: none -> 154 us  [shards(): lax.ppermute(ring[-1], 'fs', [(dev, (dev + 1) % 4) for dev in range(4)])]
    all_gather x1 -> x0, waiting for transfers between devices: 107 us -> none  [shards(): down_full = lax.all_gather(down_projection, 'fs', axis=0, tiled=True)]
    all_gather x1, waiting for transfers between devices: 104 us -> 0.01 us  [shards(): lax.all_gather(gate_projection, 'fs', axis=0, tiled=True)]
    ppermute x0 -> x3, starting transfers between devices: none -> 36.7 us  [shards(): lax.ppermute(ring[-1], 'fs', [(dev, (dev + 1) % 4) for dev in range(4)])]
    all_gather x1, waiting for transfers between devices: 99.9 us -> 73.9 us  [shards(): lax.all_gather(up_projection, 'fs', axis=0, tiled=True)]
    all_gather x1, waiting for transfers between devices: 22.4 us -> 0.01 us  [shards(): lax.all_gather(norm_rows(residual, feedforward_norm_gain).astype(jnp.bflo...]
    unnamed x21 -> x30, local copies, waits for them, and re-layouts: 3.2 us -> 17.5 us
  transfers between devices with their start and end apart: 11 -> 13, of which waited for: 10 -> 10; matrix products, arithmetic and copies ran while one was open for 20% -> 24% of each run, Pallas kernels for 0% -> 0%
where the time goes in v1:
time: 626 us; the launch traced here: 623 us
  waiting for transfers between devices  399 us (64%)
  matrix products  104 us (17%)
  local copies, waits for them, and re-layouts  59.5 us (10%)
  starting transfers between devices  37.1 us (6%)
  between operations  13.8 us (2%)
  other arithmetic  8.82 us (1%)
    ppermute x3, waiting for transfers between devices, shards(): lax.ppermute(ring[-1], 'fs', [(dev, (dev + 1) % 4) for dev in range(4)])  154 us
    all_gather x1, waiting for transfers between devices, shards(): lax.all_gather(up_projection, 'fs', axis=0, tiled=True)  73.9 us
    all_gather x1, waiting for transfers between devices, shards(): lax.all_gather(value_projection, 'fs', axis=0, tiled=True)  38.8 us
    ppermute x3, starting transfers between devices, shards(): lax.ppermute(ring[-1], 'fs', [(dev, (dev + 1) % 4) for dev in range(4)])  36.7 us
    reduce_scatter x1, waiting for transfers between devices, shards(): lax.psum_scatter(jnp.dot(headed, out_full, preferred_element_type=jnp.flo...  29.5 us
    reduce_scatter x1, waiting for transfers between devices, shards(): lax.psum_scatter(jnp.dot(hidden, down_full, preferred_element_type=jnp.fl...  29.5 us
    all_gather x1, waiting for transfers between devices, shards(): lax.all_gather(query_projection, 'fs', axis=0, tiled=True)  24 us
    all_gather x1, waiting for transfers between devices, shards(): return lax.all_gather(finished, 'tp', axis=0, tiled=True)  22.7 us
  transfers between devices with their start and end apart: 13, of which 10 were waited for; matrix products, arithmetic and copies ran while one was open for 24% of the time, Pallas kernels for 0%

profile of v1, /device:TPU:0, one launch (start us, length us, event | category | flops | bytes accessed | tf_op | source)
XLA Modules:
  0.0 622.7 jit_solution(5781928985703378375)
XLA Ops:
  9.4 2.1 fusion.62
  11.6 2.0 fusion.79
  14.8 2.7 rev.18
  17.5 22.1 %all-gather.9.cloned.1.call-done = bf16[2048,256]{1,0:T(8,128)(2,1)} async-done(((bf16[512,256]{1,0:T(8,128)(2,1)}), bf16[2048,256]{1,0:T(8,128)(2,1)}) %all-gather.9.cloned.1.call-update) | async-done | bytes 1048592 | tf_op jit(solution)/shard_map/all_gather | solution.py:84
  39.7 2.1 convolution_convert_fusion.3
  42.0 2.6 rev.19
  44.6 24.0 %all-gather.13.cloned.1.call-done = bf16[2048,256]{1,0:T(8,128)(2,1)} async-done(((bf16[512,256]{1,0:T(8,128)(2,1)}), bf16[2048,256]{1,0:T(8,128)(2,1)}) %all-gather.13.cloned.1.call-update) | async-done | bytes 1048592 | tf_op jit(solution)/shard_map/all_gather | solution.py:83
  68.6 2.1 convolution_convert_fusion.2
  71.7 4.7 rev.21
  76.5 38.8 %all-gather.11.cloned.1.call-done = bf16[2048,512]{1,0:T(8,128)(2,1)} async-done(((bf16[512,512]{1,0:T(8,128)(2,1)}), bf16[2048,512]{1,0:T(8,128)(2,1)}) %all-gather.11.cloned.1.call-update) | async-done | bytes 2097168 | tf_op jit(solution)/shard_map/all_gather | solution.py:85
  115.3 3.8 convolution_convert_fusion.1
  120.3 5.2 rev.20
  126.5 51.8 %while.27 = (s32[]{:T(128)}, f32[2,128,256]{2,1,0:T(8,128)S(1)}, f32[8,2,64,256]{3,2,0,1:T(8,128)}, f32[8,2,64,128]{3,2,0,1:T(8,128)}, f32[8,2,64,128]{3,2,0,1:T...) while((s32[]{:T(128)}, f32[2,128,256]{2,1,0:T(8,128)S(1)}, ...), condition=%wide.region_6.7_spmd.clone, body=%wide.region_4.6_spmd.clone.sunk | while | flops 139866112 | bytes 2320003 | solution.py:46
  178.5 31.7 %while.26 = (s32[]{:T(128)}, f32[2,128,256]{2,1,0:T(8,128)S(1)}, f32[8,2,64,256]{3,2,0,1:T(8,128)S(1)}, f32[8,2,64,128]{3,2,0,1:T(8,128)}, f32[8,2,64,128]{3,2,0...) while((s32[]{:T(128)}, f32[2,128,256]{2,1,0:T(8,128)S(1)}, ...), condition=%wide.region_3.4_spmd.clone, body=%wide.region_1.3_spmd.clone.sunk | while | flops 139866112 | bytes 2352771 | solution.py:46
  210.2 6.8 %rev.22 = f32[2,512,256]{2,1,0:T(8,128)S(1)} reverse(f32[2,512,256]{2,1,0:T(8,128)} %bitcast.195), dimensions={1} | reverse | bytes 2097152 | tf_op jit(solution)/shard_map/vmap(jit(_flip))/rev | solution.py:55
  217.9 4.2 convolution_convert_fusion
  222.7 29.5 %reduce-scatter.3.cloned.1.call-done = bf16[128,2048]{1,0:T(8,128)(2,1)} async-done(((bf16[512,2048]{1,0:T(8,128)(2,1)}), bf16[128,2048]{1,0:T(8,128)(2,1)}) %reduce-scatter.3.cloned.1.call-update) | async-done | bytes 524304 | tf_op jit(solution)/shard_map/reduce_scatter | solution.py:118
  257.1 58.4 %collective-permute-done = bf16[352,2048]{1,0:T(8,128)(2,1)S(1)} collective-permute-done((bf16[352,2048]{1,0:T(8,128)(2,1)S(1)}, bf16[352,2048]{1,0:T(8,128)(2,1)S(1)}, u32[]{:S(2)}, u32[]{:S(2)}) %collective-permute-start) | collective-permute-done | bytes 1441824 | tf_op jit(solution)/shard_map/ppermute | solution.py:138
  315.5 27.0 %collective-permute-start.1 = (bf16[352,2048]{1,0:T(8,128)(2,1)S(1)}, bf16[352,2048]{1,0:T(8,128)(2,1)}, u32[]{:S(2)}, u32[]{:S(2)}) collective-permute-start(bf16[352,2048]{1,0:T(8,128)(2,1)S(1)} %collective-permute-done), channel_id=1, source_target_pairs={{0,4},{4,8},{8,12},{12,0},{1,5},{5,9},{9,13},{13,1},{2,6},{6,10},{... | collective-permute-start | bytes 4325384 | tf_op jit(solution)/shard_map/ppermute | solution.py:138
  342.6 62.2 %collective-permute-done.1 = bf16[352,2048]{1,0:T(8,128)(2,1)} collective-permute-done((bf16[352,2048]{1,0:T(8,128)(2,1)S(1)}, bf16[352,2048]{1,0:T(8,128)(2,1)}, u32[]{:S(2)}, u32[]{:S(2)}) %collective-permute-start.1) | collective-permute-done | bytes 1441824 | tf_op jit(solution)/shard_map/ppermute | solution.py:138
  404.8 8.1 %collective-permute-start.2 = (bf16[352,2048]{1,0:T(8,128)(2,1)}, bf16[352,2048]{1,0:T(8,128)(2,1)}, u32[]{:S(2)}, u32[]{:S(2)}) collective-permute-start(bf16[352,2048]{1,0:T(8,128)(2,1)} %collective-permute-done.1), channel_id=1, source_target_pairs={{0,4},{4,8},{8,12},{12,0},{1,5},{5,9},{9,13},{13,1},{2,6},{6,10},{... | collective-permute-start | bytes 4325384 | tf_op jit(solution)/shard_map/ppermute | solution.py:138
  412.9 33.8 %collective-permute-done.2 = bf16[352,2048]{1,0:T(8,128)(2,1)} collective-permute-done((bf16[352,2048]{1,0:T(8,128)(2,1)}, bf16[352,2048]{1,0:T(8,128)(2,1)}, u32[]{:S(2)}, u32[]{:S(2)}) %collective-permute-start.2) | collective-permute-done | bytes 1441824 | tf_op jit(solution)/shard_map/ppermute | solution.py:138
  446.6 2.7 constant_dynamic-update-slice_fusion.7
  449.3 2.6 constant_dynamic-update-slice_fusion.6
  454.4 2.6 constant_dynamic-update-slice_fusion.3
  457.1 2.7 constant_dynamic-update-slice_fusion.2
  462.2 8.4 %fusion.89 = f32[512,1408]{1,0:T(8,128)} fusion(bf16[512,2048]{1,0:T(8,128)(2,1)} %all-gather.17.cloned.1.call-done, bf16[2048,1408]{1,0:T(8,128)(2,1)} %all-gather.19.cloned.1.call-done), kind=kOutput, calls=%fused_computation.126 | convolution fusion | flops 2952790016 | bytes 10747904 | tf_op jit(solution)/shard_map/dot_general | solution.py:133
  470.5 73.9 %all-gather.21.cloned.1.call-done = bf16[2048,1408]{1,0:T(8,128)(2,1)} async-done(((bf16[512,1408]{1,0:T(8,128)(2,1)}), bf16[2048,1408]{1,0:T(8,128)(2,1)}) %all-gather.21.cloned.1.call-update) | async-done | bytes 5767184 | tf_op jit(solution)/shard_map/all_gather | solution.py:131
  544.4 14.0 %fusion.66 = bf16[512,2048]{1,0:T(8,128)(2,1)} fusion(bf16[2816,2048]{1,0:T(8,128)(2,1)} %constant_dynamic-update-slice_fusion, s32[]{:T(128)S(6)} %select_n.31, bf16[512,2048]{1,0:T(8,128)(2,1)} %all-gather.17.cloned.1.call-done, bf16[2048,1408]{1,0:T(8,128)(2,1)} %all-gather.21.cloned.1.call-done, f32[512,1408]{1,0:T(8,128)} %fusion.89), kind=kOutput, calls=%fused_computation.85 | convolution fusion | flops 5910953984 | bytes 18612228 | tf_op jit(solution)/shard_map/dot_general | solution.py:143
  558.5 29.5 %reduce-scatter.5.cloned.1.call-done = bf16[128,2048]{1,0:T(8,128)(2,1)} async-done(((bf16[512,2048]{1,0:T(8,128)(2,1)}), bf16[128,2048]{1,0:T(8,128)(2,1)}) %reduce-scatter.5.cloned.1.call-update) | async-done | bytes 524304 | tf_op jit(solution)/shard_map/reduce_scatter | solution.py:142
  590.0 22.7 %all-gather.23.cloned.1.call-done = bf16[512,2048]{1,0:T(8,128)(2,1)} async-done(((bf16[128,2048]{1,0:T(8,128)(2,1)}), bf16[512,2048]{1,0:T(8,128)(2,1)}) %all-gather.23.cloned.1.call-update) | async-done | bytes 2097168 | tf_op jit(solution)/shard_map/all_gather | solution.py:149
  612.7 3.2 copy.80
  (212 shorter events, 103.2 us)
Async XLA Ops:
  6.5 5.0 copy-start
  6.5 5.0 copy-start.2
  6.5 5.0 copy-start.5
  6.5 5.0 copy-start.8
  6.5 5.0 copy-start.9
  6.5 5.0 copy-start.6
  6.6 33.1 %all-gather.9.cloned.1.call-start = ((), (), s32[]{:S(2)}) async-start(), calls=%async_computation.2 | async-start | bytes 1310720 | tf_op jit(solution)/shard_map/all_gather | solution.py:84
  7.3 61.3 %all-gather.13.cloned.1.call-start = ((), (), s32[]{:S(2)}) async-start(), calls=%async_computation.4 | async-start | bytes 1310720 | tf_op jit(solution)/shard_map/all_gather | solution.py:83
  8.0 107.2 %all-gather.11.cloned.1.call-start = ((), (), s32[]{:S(2)}) async-start(), calls=%async_computation.3 | async-start | bytes 2621440 | tf_op jit(solution)/shard_map/all_gather | solution.py:85
  8.8 209.1 %all-gather.15.cloned.1.call-start = ((), (), s32[]{:S(2)}) async-start(), calls=%async_computation.5 | async-start | bytes 2621440 | tf_op jit(solution)/shard_map/all_gather | solution.py:117
  9.4 242.9 %reduce-scatter.3.cloned.1.call-start = ((), (), s32[]{:S(2)}) async-start(), calls=%async_computation.6 | async-start | bytes 2621440 | tf_op jit(solution)/shard_map/reduce_scatter | solution.py:118
  14.8 27.0 %copy-start.4 = (f32[512,2,128]{2,0,1:T(8,128)}, f32[512,2,128]{2,0,1:T(8,128)S(1)}, u32[]{:S(2)}) copy-start(f32[512,2,128]{2,0,1:T(8,128)S(1)} %copy.16) | copy-start | bytes 1572868
  210.2 7.2 %copy-start.10 = (f32[256]{0:T(256)S(1)}, f32[256]{0:T(256)}, u32[]{:S(2)}) copy-start(f32[256]{0:T(256)} %param.28) | copy-start | bytes 3076
  222.1 31.7 %copy-start.7 = (f32[2048]{0:T(1024)S(1)}, f32[2048]{0:T(1024)}, u32[]{:S(2)}) copy-start(f32[2048]{0:T(1024)} %param.30) | copy-start | bytes 24580
  222.1 33.5 %copy-start.3 = (bf16[352,2048]{1,0:T(8,128)(2,1)S(1)}, bf16[352,2048]{1,0:T(8,128)(2,1)}, u32[]{:S(2)}) copy-start(bf16[352,2048]{1,0:T(8,128)(2,1)} %param.33) | copy-start | bytes 4325380
  222.1 240.1 %all-gather.19.cloned.1.call-start = ((), (), s32[]{:S(2)}) async-start(), calls=%async_computation.8 | async-start | bytes 7208960 | tf_op jit(solution)/shard_map/all_gather | solution.py:130
  222.7 239.5 %all-gather.17.cloned.1.call-start = ((), (), s32[]{:S(2)}) async-start(), calls=%async_computation.7 | async-start | bytes 2621440 | tf_op jit(solution)/shard_map/all_gather | solution.py:126
  254.7 289.7 %all-gather.21.cloned.1.call-start = ((), (), s32[]{:S(2)}) async-start(), calls=%async_computation.9 | async-start | bytes 7208960 | tf_op jit(solution)/shard_map/all_gather | solution.py:131
  255.5 332.5 %reduce-scatter.5.cloned.1.call-start = ((), (), s32[]{:S(2)}) async-start(), calls=%async_computation.10 | async-start | bytes 2621440 | tf_op jit(solution)/shard_map/reduce_scatter | solution.py:142
  255.6 60.0 %collective-permute-start = (bf16[352,2048]{1,0:T(8,128)(2,1)S(1)}, bf16[352,2048]{1,0:T(8,128)(2,1)S(1)}, u32[]{:S(2)}, u32[]{:S(2)}) collective-permute-start(bf16[352,2048]{1,0:T(8,128)(2,1)S(1)} %copy-done.3), channel_id=1, source_target_pairs={{0,4},{4,8},{8,12},{12,0},{1,5},{5,9},{9,13},{13,1},{2,6},{6,10},{... | collective-permute-start | bytes 4325384 | tf_op jit(solution)/shard_map/ppermute | solution.py:138
  315.5 89.3 %collective-permute-start.1 = (bf16[352,2048]{1,0:T(8,128)(2,1)S(1)}, bf16[352,2048]{1,0:T(8,128)(2,1)}, u32[]{:S(2)}, u32[]{:S(2)}) collective-permute-start(bf16[352,2048]{1,0:T(8,128)(2,1)S(1)} %collective-permute-done), channel_id=1, source_target_pairs={{0,4},{4,8},{8,12},{12,0},{1,5},{5,9},{9,13},{13,1},{2,6},{6,10},{... | collective-permute-start | bytes 4325384 | tf_op jit(solution)/shard_map/ppermute | solution.py:138
  404.8 41.9 %collective-permute-start.2 = (bf16[352,2048]{1,0:T(8,128)(2,1)}, bf16[352,2048]{1,0:T(8,128)(2,1)}, u32[]{:S(2)}, u32[]{:S(2)}) collective-permute-start(bf16[352,2048]{1,0:T(8,128)(2,1)} %collective-permute-done.1), channel_id=1, source_target_pairs={{0,4},{4,8},{8,12},{12,0},{1,5},{5,9},{9,13},{13,1},{2,6},{6,10},{... | collective-permute-start | bytes 4325384 | tf_op jit(solution)/shard_map/ppermute | solution.py:138
  558.4 57.4 %copy-start.1 = (bf16[2048,16]{0,1:T(8,128)(2,1)S(1)}, bf16[2048,16]{0,1:T(8,128)(2,1)}, u32[]{:S(2)}) copy-start(bf16[2048,16]{0,1:T(8,128)(2,1)} %param.24) | copy-start | bytes 196612
  558.5 54.2 %all-gather.23.cloned.1.call-start = ((), (), s32[]{:S(2)}) async-start(), calls=%async_computation.11 | async-start | bytes 2621440 | tf_op jit(solution)/shard_map/all_gather | solution.py:149
Sparse Core Ops, SparseCore 0:
  8.9 30.6 all-gather.8
  41.2 27.3 all-gather.12
  70.2 45.0 all-gather.10
  116.7 44.5 all-gather.14
  222.2 29.9 reduce-scatter.2
  253.7 160.9 all-gather.18
  416.3 19.8 all-gather.16
  437.7 106.6 all-gather.20
  558.6 29.3 reduce-scatter.4
  590.1 22.5 all-gather.22
